TPU v7x, 32 devices: a whole 2x2x4 slice. The times are simulated.
32 devices in a mesh: sp: 8 (over z, x), tp: 4 (over y, core).
Axes of the slice: x: 2, y: 2, z: 4, core: 2. Of those that a mesh axis runs over, the one named last changes fastest.
Arguments:
- query_wide: bfloat16 [1024, 1536], P('sp', 'tp'), may hold values from -600 to 600
- query_narrow: bfloat16 [1024, 1024], P('sp', 'tp'), may hold values from -600 to 600
- latent: bfloat16 [1024, 512], P('sp'), may hold values from -6 to 6
- rope_key: bfloat16 [1024, 64], P('sp'), may hold values from -6 to 6
- latent_norm_weight: float32 [512], replicated, may hold values from 0.1 to 1.9
- broad_key_lift: bfloat16 [512, 1024], P(None, 'tp'), may hold values from -0.25 to 0.25
- broad_value_lift: bfloat16 [512, 1024], P(None, 'tp'), may hold values from -0.25 to 0.25
- slim_key_lift: bfloat16 [512, 512], P(None, 'tp'), may hold values from -0.25 to 0.25
- slim_value_lift: bfloat16 [512, 512], P(None, 'tp'), may hold values from -0.25 to 0.25
- out_wide: bfloat16 [1024, 2048], P('tp'), may hold values from -0.4375 to 0.4375
- out_narrow: bfloat16 [512, 2048], P('tp'), may hold values from -0.4375 to 0.4375
- resid: bfloat16 [1024, 2048], P('sp'), may hold values from -20 to 20
- ffn_gain: float32 [2048], replicated, may hold values from 0.1 to 1.9
- group_route: int32 [1024], P('sp'), may hold values from 0 to 7, as said below
- expert_pair: int32 [1024, 2], P('sp'), may hold values from 0 to 3, all different within a row
- group_prob: float32 [1024], P('sp'), may hold values from 0.2 to 1
- expert_prob: float32 [1024, 2], P('sp'), may hold values from 0.05 to 1
- gate_weight: bfloat16 [8, 4, 2048, 512], P('sp', None, None, 'tp'), may hold values from -0.125 to 0.125
- up_weight: bfloat16 [8, 4, 2048, 512], P('sp', None, None, 'tp'), may hold values from -0.125 to 0.125
- down_weight: bfloat16 [8, 4, 512, 2048], P('sp', None, 'tp'), may hold values from -0.25 to 0.25
Outputs:
- mixed: bfloat16 [1024, 2048], P('sp', 'tp')
Inputs may be any that keep to these rules, and one draw needn't show every extreme that they name: `group_route`: of the 128 tokens of one index of sp at most 32 name one group; in every draw one group is named by exactly 32 tokens of every index of sp, and every index of sp names one more group exactly 32 times. `expert_pair`: A token's two experts are different.
All inputs are finite; a program needn't handle non-finite values.
Results may differ from a plain program's by a relative error of at most 0.017.
Values may be sent and summed in bfloat16 or wider, within the bound.
A program may use at most 128 MiB of HBM per device.

v0:
```python
import math
import jax
import jax.numpy as jnp
from jax import lax
from jax.sharding import PartitionSpec as P

PLAIN_WIDTH_WIDE = 128
PLAIN_WIDTH_SLIM = 64
ROPE = 64
VALUE_WIDTH_WIDE = 128
VALUE_WIDTH_SLIM = 64
EPG = 4
ROPE_BASE = 10000.0
EPSILON = 1e-06
MASKED = -1e30


def rms_scale(values, gain_row):
    widened = values.astype(jnp.float32)
    return (
        widened
        * lax.rsqrt(jnp.mean(widened * widened, axis=-1, keepdims=True) + EPSILON)
        * gain_row
    )


def angles(positions, width):
    frequency = 1.0 / ROPE_BASE ** (jnp.arange(0, width, 2).astype(jnp.float32) / width)
    return positions.astype(jnp.float32)[:, None] * frequency[None, :]


def rotary(values, angle_table):
    half_width = values.shape[-1] // 2
    first_half = values[..., :half_width]
    second = values[..., half_width:]
    return jnp.concatenate(
        [
            first_half * jnp.cos(angle_table) - second * jnp.sin(angle_table),
            second * jnp.cos(angle_table) + first_half * jnp.sin(angle_table),
        ],
        axis=-1,
    )


def split_query(queries, head_count, nope_width, angle_table):
    shaped = queries.reshape(queries.shape[0], head_count, nope_width + ROPE)
    turned = rotary(shaped[..., nope_width:].astype(jnp.float32), angle_table[:, None, :]).astype(
        jnp.bfloat16
    )
    return (shaped[..., :nope_width], turned)


def group_step(
    carry_state, query_pair, key_block, value_block, rot_block, key_pos, query_pos, scale
):
    row_peak, row_total, accum_out = carry_state
    scores = jnp.einsum(
        "thd,khd->htk", query_pair[0], key_block, preferred_element_type=jnp.float32
    )
    scores = scores + jnp.einsum(
        "thd,kd->htk", query_pair[1], rot_block, preferred_element_type=jnp.float32
    )
    scores = jnp.where((query_pos[:, None] >= key_pos[None, :])[None], scores * scale, MASKED)
    new_peak = jnp.maximum(row_peak, jnp.max(scores, axis=-1))
    keep_factor = jnp.exp(row_peak - new_peak)
    weights = jnp.exp(scores - new_peak[:, :, None])
    row_total = row_total * keep_factor + jnp.sum(weights, axis=-1)
    accum_out = accum_out * keep_factor.T[:, :, None] + jnp.einsum(
        "htk,khd->thd",
        weights.astype(jnp.bfloat16),
        value_block,
        preferred_element_type=jnp.float32,
    )
    return (new_peak, row_total, accum_out)


def empty_state(head_count, width, local_tokens):
    return (
        jnp.full((head_count, local_tokens), MASKED, jnp.float32),
        jnp.zeros((head_count, local_tokens), jnp.float32),
        jnp.zeros((local_tokens, head_count, width), jnp.float32),
    )


def finish(carry_state):
    normalized = carry_state[2] / carry_state[1].T[:, :, None]
    return normalized.astype(jnp.bfloat16).reshape(normalized.shape[0], -1)


def project(latent_rows, weight):
    return jnp.dot(latent_rows, weight, preferred_element_type=jnp.float32).astype(jnp.bfloat16)


def body(
    query_wide,
    query_narrow,
    latent,
    rope_key,
    latent_norm_weight,
    broad_key_lift,
    broad_value_lift,
    slim_key_lift,
    slim_value_lift,
    out_wide,
    out_narrow,
    resid,
    ffn_gain,
    group_route,
    expert_pair,
    group_prob,
    expert_prob,
    gate_weight,
    up_weight,
    down_weight,
):
    local_tokens = latent.shape[0]
    offset = lax.axis_index("sp") * local_tokens
    query_pos = offset + jnp.arange(local_tokens, dtype=jnp.int32)
    angle_table = angles(query_pos, ROPE)
    latent_rows = rms_scale(latent, latent_norm_weight).astype(jnp.bfloat16)
    rot_key = rotary(rope_key.astype(jnp.float32), angle_table).astype(jnp.bfloat16)
    heads_wide = query_wide.shape[1] // (PLAIN_WIDTH_WIDE + ROPE)
    heads_narrow = query_narrow.shape[1] // (PLAIN_WIDTH_SLIM + ROPE)
    wide_query = split_query(query_wide, heads_wide, PLAIN_WIDTH_WIDE, angle_table)
    narrow_query = split_query(query_narrow, heads_narrow, PLAIN_WIDTH_SLIM, angle_table)

    def expand(lat_block):
        return (
            project(lat_block, broad_key_lift),
            project(lat_block, broad_value_lift),
            project(lat_block, slim_key_lift),
            project(lat_block, slim_value_lift),
        )

    def attend(carry_state, key_set, key_pos):
        key_w, value_w, key_n, value_n, rot_block = key_set
        block_rows = rot_block.shape[0]
        wide_state = group_step(
            carry_state[0],
            wide_query,
            key_w.reshape(block_rows, heads_wide, PLAIN_WIDTH_WIDE),
            value_w.reshape(block_rows, heads_wide, VALUE_WIDTH_WIDE),
            rot_block,
            key_pos,
            query_pos,
            (PLAIN_WIDTH_WIDE + ROPE) ** (-0.5),
        )
        narrow_state = group_step(
            carry_state[1],
            narrow_query,
            key_n.reshape(block_rows, heads_narrow, PLAIN_WIDTH_SLIM),
            value_n.reshape(block_rows, heads_narrow, VALUE_WIDTH_SLIM),
            rot_block,
            key_pos,
            query_pos,
            (PLAIN_WIDTH_SLIM + ROPE) ** (-0.5),
        )
        return (wide_state, narrow_state)

    start_state = (
        empty_state(heads_wide, VALUE_WIDTH_WIDE, local_tokens),
        empty_state(heads_narrow, VALUE_WIDTH_SLIM, local_tokens),
    )
    pieces = (
        lax.all_gather(latent_rows, "sp", axis=0, tiled=True),
        lax.all_gather(rot_key, "sp", axis=0, tiled=True),
    )
    total_rows = pieces[0].shape[0]
    block_rows = math.gcd(total_rows, 1024)

    def visit_block(block_index, carry_inner):
        block_start = block_index * block_rows
        sliced = tuple(
            (lax.dynamic_slice_in_dim(piece, block_start, block_rows, 0) for piece in pieces)
        )
        key_pos = block_start + jnp.arange(block_rows, dtype=jnp.int32)

        def work_block(running):
            key_set = expand(sliced[0]) + (sliced[1],)
            return attend(running, key_set, key_pos)

        return lax.cond(
            block_start > query_pos[-1], lambda unchanged: unchanged, work_block, carry_inner
        )

    final_state = lax.fori_loop(0, total_rows // block_rows, visit_block, start_state)
    att_wide = finish(final_state[0])
    att_narrow = finish(final_state[1])
    partial_value = jnp.dot(att_wide, out_wide, preferred_element_type=jnp.float32)
    partial_value = partial_value + jnp.dot(
        att_narrow, out_narrow, preferred_element_type=jnp.float32
    )
    model_width = resid.shape[1]
    tp_size = lax.axis_size("tp")
    quarter = model_width // tp_size
    col_start = lax.axis_index("tp") * quarter
    summed = lax.psum(partial_value.astype(jnp.bfloat16), "tp").astype(jnp.float32)
    stream = (resid.astype(jnp.float32) + summed).astype(jnp.bfloat16)
    normed = rms_scale(stream, ffn_gain).astype(jnp.bfloat16)
    stream_cols = lax.dynamic_slice_in_dim(stream, col_start, quarter, 1)
    groups = lax.axis_size("sp")
    capacity = 2 * local_tokens // groups
    share_of = group_prob[:, None] * expert_prob / jnp.sum(expert_prob, axis=1, keepdims=True)
    chosen = (expert_pair[:, :, None] == jnp.arange(EPG, dtype=jnp.int32)[None, None, :]).astype(
        jnp.float32
    )
    combine = jnp.sum(share_of[:, :, None] * chosen, axis=1).astype(jnp.bfloat16)
    member = (group_route[:, None] == jnp.arange(groups, dtype=jnp.int32)[None, :]).astype(
        jnp.int32
    )
    group_rank = jnp.sum(jnp.cumsum(member, axis=0) * member, axis=1) - 1
    slot_index = group_route * capacity + group_rank
    routed_weights = jnp.zeros((groups * capacity, EPG), jnp.bfloat16).at[slot_index].set(combine)
    routed_weights = routed_weights.reshape(groups, capacity, EPG)
    column_rows = lax.dynamic_slice_in_dim(normed, col_start, quarter, 1)
    placed = (
        jnp.zeros((groups * capacity, column_rows.shape[1]), jnp.bfloat16)
        .at[slot_index]
        .set(column_rows)
    )
    joined = lax.all_gather(
        lax.all_to_all(
            placed.reshape(groups, capacity, column_rows.shape[1]),
            "sp",
            split_axis=0,
            concat_axis=0,
            tiled=True,
        ),
        "tp",
        axis=2,
        tiled=True,
    )
    slot_count = joined.shape[0] * joined.shape[1]
    flat_rows = joined.reshape(slot_count, joined.shape[2])
    gate_act = jnp.einsum(
        "rd,edf->ref", flat_rows, gate_weight[0], preferred_element_type=jnp.float32
    )
    up_act = jnp.einsum("rd,edf->ref", flat_rows, up_weight[0], preferred_element_type=jnp.float32)
    scaled = (
        lax.all_to_all(routed_weights, "sp", split_axis=0, concat_axis=0, tiled=True)
        .reshape(slot_count, EPG)
        .astype(jnp.float32)[:, :, None]
    )
    hidden = (jax.nn.silu(gate_act) * up_act * scaled).astype(jnp.bfloat16)
    partials = jnp.einsum("ref,efd->rd", hidden, down_weight[0], preferred_element_type=jnp.float32)
    partials = partials.reshape(joined.shape)
    summed_rows = lax.psum_scatter(
        partials.astype(jnp.bfloat16), "tp", scatter_dimension=2, tiled=True
    )
    returned_rows = lax.all_to_all(summed_rows, "sp", split_axis=0, concat_axis=0, tiled=True)
    moe_rows = returned_rows.reshape(groups * capacity, quarter)[slot_index]
    return (stream_cols.astype(jnp.float32) + moe_rows.astype(jnp.float32)).astype(jnp.bfloat16)


def solution(mesh):
    placed = (
        P("sp", "tp"),
        P("sp", "tp"),
        P("sp", None),
        P("sp", None),
        P(),
        P(None, "tp"),
        P(None, "tp"),
        P(None, "tp"),
        P(None, "tp"),
        P("tp", None),
        P("tp", None),
        P("sp", None),
        P(),
        P("sp"),
        P("sp", None),
        P("sp"),
        P("sp", None),
        P("sp", None, None, "tp"),
        P("sp", None, None, "tp"),
        P("sp", None, "tp", None),
    )
    return jax.shard_map(body, mesh=mesh, in_specs=placed, out_specs=P("sp", "tp"), check_vma=False)
```

profile of v0, /device:TPU:0, one launch (start us, length us, event | category | flops | bytes accessed | tf_op | source)
XLA Modules:
  0.0 180.7 jit_solution(8999266724435186518)
XLA Ops:
  6.5 1.2 fusion.38
  7.7 1.7 fusion.40
  9.5 0.7 convert_element_type.130
  10.2 1.0 copy.74
  11.2 1.0 copy.75
  12.2 0.6 slice.38
  13.5 0.7 fusion.48
  14.6 28.3 %all_gather.10 = bf16[1024,64]{0,1:T(8,128)(2,1)S(1)} all-gather(bf16[128,64]{0,1:T(8,128)(2,1)S(1)} %pad_maximum_fusion.2), channel_id=1, replica_groups=mesh['sp'=8,'tp'=4] {'sp'}, dimensions={0}, use_global_device_ids=true | all-gather | bytes 147456 | tf_op jit(solution)/shard_map/all_gather | solution.py:166
  43.0 0.6 pad_maximum_fusion
  43.6 9.6 %all-gather.3.cloned.1.call-done = bf16[1024,512]{1,0:T(8,128)(2,1)} async-done(((bf16[128,512]{1,0:T(8,128)(2,1)}), bf16[1024,512]{1,0:T(8,128)(2,1)}) %all-gather.3.cloned.1.call-update) | async-done | bytes 1048592 | tf_op jit(solution)/shard_map/all_gather | solution.py:165
  53.2 7.1 %conditional.1 = (f32[2,128]{1,0:T(2,128)S(1)}, f32[128,2,128]{0,2,1:T(8,128)S(1)}, f32[2,128]{1,0:T(2,128)S(1)}, f32[128,2,64]{0,2,1:T(8,128)S(1)}) conditional(s32[]{:T(128)} %bitcast.13, (s32[128]{0:T(128)S(1)}, s32[1024]{0:T(1024)S(1)}, bf16[1024,512]{1,0:T(8,128)(2,1)}, bf16[512,256]{1,0:T(8,128)(2,1)S(1)}, bf16[128,2,192]{0,2,1:T(8,128)(2,1)S(1)}, ...), branch_computations={%region_1.6_spmd, %region_6.7_spmd} | conditional | flops 1078953472 | bytes 26996452 | solution.py:182
  53.2 0.6 copy-done.6
  53.8 1.7 convolution_convert_fusion.1
  60.4 1.6 fusion.54
  62.0 1.1 fusion.23
  63.4 0.8 dynamic-slice
  64.2 31.1 %all-reduce.2.cloned.1.call-done = bf16[128,2048]{1,0:T(8,128)(2,1)} async-done(((bf16[128,2048]{1,0:T(8,128)(2,1)}), bf16[128,2048]{1,0:T(8,128)(2,1)}) %all-reduce.2.cloned.1.call-update) | async-done | bytes 524304 | tf_op jit(solution)/shard_map/psum | solution.py:197
  95.3 1.3 multiply_reduce_fusion
  96.6 1.1 convert_element_type.142
  97.7 1.6 scatter_custom_fusion
  99.3 13.6 %all_to_all.15 = bf16[8,32,512]{2,1,0:T(8,128)(2,1)} all-to-all(bf16[8,32,512]{2,1,0:T(8,128)(2,1)S(1)} %bitcast.107), channel_id=1, replica_groups=mesh['sp'=8,'tp'=4] {'sp'}, dimensions={0} | all-to-all | bytes 524288 | tf_op jit(solution)/shard_map/all_to_all | solution.py:222
  113.2 0.9 scatter_custom_fusion.1
  114.2 9.7 %all_to_all.16 = bf16[8,32,4]{1,2,0:T(4,128)(2,1)S(1)} all-to-all(bf16[8,32,4]{1,2,0:T(4,128)(2,1)S(1)} %copy.78), channel_id=1, replica_groups=mesh['sp'=8,'tp'=4] {'sp'}, dimensions={0} | all-to-all | bytes 4096 | tf_op jit(solution)/shard_map/all_to_all | solution.py:240
  124.0 4.1 %all-gather.5.cloned.1.call-done = bf16[8,32,2048]{2,1,0:T(8,128)(2,1)} async-done(((bf16[8,32,512]{2,1,0:T(8,128)(2,1)}), bf16[8,32,2048]{2,1,0:T(8,128)(2,1)}) %all-gather.5.cloned.1.call-update) | async-done | bytes 1048592 | tf_op jit(solution)/shard_map/all_gather | solution.py:221
  128.1 2.8 %fusion.27 = f32[256,4,128]{2,0,1:T(8,128)S(1)} fusion(bf16[256,2048,1]{1,0,2:T(8,128)(2,1)} %bitcast.119, bf16[1,4,2048,128]{3,2,1,0:T(8,128)(2,1)} %param.39), kind=kOutput, calls=%fused_computation.49 | convolution fusion | flops 536870912 | bytes 3670016 | tf_op jit(solution)/shard_map/rd,edf->ref/dot_general | solution.py:235
  130.9 0.7 fusion.35
  131.7 1.7 fusion.22
  133.4 24.9 %reduce-scatter.2.cloned.1.call-done = bf16[8,32,512]{2,1,0:T(8,128)(2,1)} async-done(((bf16[8,32,2048]{2,1,0:T(8,128)(2,1)}), bf16[8,32,512]{2,1,0:T(8,128)(2,1)}) %reduce-scatter.2.cloned.1.call-update) | async-done | bytes 262160 | tf_op jit(solution)/shard_map/reduce_scatter | solution.py:247
  158.3 5.5 %all-to-all-start.2 = ((bf16[8,32,512]{2,1,0:T(8,128)(2,1)}), bf16[8,32,512]{2,1,0:T(8,128)(2,1)S(1)}, u32[]{:S(2)}, u32[]{:S(2)}) async-start(bf16[8,32,512]{2,1,0:T(8,128)(2,1)} %reduce-scatter.2.cloned.1.call-done), calls=%async_computation.3 | async-start | bytes 524288 | tf_op jit(solution)/shard_map/all_to_all | solution.py:250
  163.9 8.7 %all-to-all-done.2 = bf16[8,32,512]{2,1,0:T(8,128)(2,1)S(1)} async-done(((bf16[8,32,512]{2,1,0:T(8,128)(2,1)}), bf16[8,32,512]{2,1,0:T(8,128)(2,1)S(1)}, u32[]{:S(2)}, u32[]{:S(2)}) %all-to-all-start.2) | async-done | bytes 262176 | tf_op jit(solution)/shard_map/all_to_all | solution.py:250
  172.6 0.8 gather_fusion
  173.4 0.7 add_convert_fusion.1
  (83 shorter events, 5.9 us)
Async XLA Ops:
  6.5 125.1 %copy-start = (bf16[1,4,128,2048]{3,2,1,0:T(8,128)(2,1)S(1)}, bf16[1,4,128,2048]{3,2,1,0:T(8,128)(2,1)}, u32[]{:S(2)}) copy-start(bf16[1,4,128,2048]{3,2,1,0:T(8,128)(2,1)} %param.41) | copy-start | bytes 6291460
  6.5 46.6 %copy-start.4 = (bf16[512,256]{1,0:T(8,128)(2,1)S(1)}, bf16[512,256]{1,0:T(8,128)(2,1)}, u32[]{:S(2)}) copy-start(bf16[512,256]{1,0:T(8,128)(2,1)} %param.27) | copy-start | bytes 786436
  6.5 46.6 %all-gather.3.cloned.1.call-start = ((), (), s32[]{:S(2)}) async-start(), calls=%async_computation.4 | async-start | bytes 1179648 | tf_op jit(solution)/shard_map/all_gather | solution.py:165
  9.4 85.8 %all-reduce.2.cloned.1.call-start = ((), (), s32[]{:S(2)}) async-start(), calls=%async_computation.5 | async-start | bytes 1048576 | tf_op jit(solution)/shard_map/psum | solution.py:197
  53.2 0.6 copy-start.6
  55.6 1.2 copy-start.1
  55.6 1.2 copy-start.9
  56.0 1.3 copy-start.7
  56.2 1.5 copy-start.8
  57.7 0.9 copy-start.10
  58.1 1.3 copy-start.5
  60.3 1.7 copy-start.3
  60.4 2.9 %copy-start.12 = (s32[128]{0:T(128)S(1)}, s32[128]{0:T(128)}, u32[]{:S(2)}) copy-start(s32[128]{0:T(128)} %param.35) | copy-start | bytes 1540
  60.4 34.9 %copy-start.2 = (bf16[128,2048]{1,0:T(8,128)(2,1)S(1)}, bf16[128,2048]{1,0:T(8,128)(2,1)}, u32[]{:S(2)}) copy-start(bf16[128,2048]{1,0:T(8,128)(2,1)} %param.33) | copy-start | bytes 1572868
  63.2 64.9 %all-gather.5.cloned.1.call-start = ((), (), s32[]{:S(2)}) async-start(), calls=%async_computation.6 | async-start | bytes 1310720 | tf_op jit(solution)/shard_map/all_gather | solution.py:221
  64.2 48.8 %copy-start.11 = (f32[128,2]{0,1:T(2,128)S(1)}, f32[128,2]{0,1:T(2,128)}, u32[]{:S(2)}) copy-start(f32[128,2]{0,1:T(2,128)} %param.38) | copy-start | bytes 3076
  64.2 48.8 %copy-start.14 = (f32[128]{0:T(128)S(1)}, f32[128]{0:T(128)}, u32[]{:S(2)}) copy-start(f32[128]{0:T(128)} %param.37) | copy-start | bytes 1540
  64.2 48.9 %copy-start.13 = (s32[128,2]{0,1:T(2,128)S(1)}, s32[128,2]{0,1:T(2,128)}, u32[]{:S(2)}) copy-start(s32[128,2]{0,1:T(2,128)} %param.36) | copy-start | bytes 3076
  112.9 45.4 %reduce-scatter.2.cloned.1.call-start = ((), (), s32[]{:S(2)}) async-start(), calls=%async_computation.7 | async-start | bytes 1310720 | tf_op jit(solution)/shard_map/reduce_scatter | solution.py:247
  128.1 2.8 %copy-start.15 = (bf16[1,4,2048,128]{3,2,1,0:T(8,128)(2,1)S(1)}, bf16[1,4,2048,128]{3,2,1,0:T(8,128)(2,1)}, u32[]{:S(2)}) copy-start(bf16[1,4,2048,128]{3,2,1,0:T(8,128)(2,1)} %param.40) | copy-start | bytes 6291460
  128.1 2.8 %copy-start.16 = (bf16[8,32,2048]{2,1,0:T(8,128)(2,1)S(1)}, bf16[8,32,2048]{2,1,0:T(8,128)(2,1)}, u32[]{:S(2)}) copy-start(bf16[8,32,2048]{2,1,0:T(8,128)(2,1)} %all-gather.5.cloned.1.call-done) | copy-start | bytes 3145732
  158.3 14.3 %all-to-all-start.2 = ((bf16[8,32,512]{2,1,0:T(8,128)(2,1)}), bf16[8,32,512]{2,1,0:T(8,128)(2,1)S(1)}, u32[]{:S(2)}, u32[]{:S(2)}) async-start(bf16[8,32,512]{2,1,0:T(8,128)(2,1)} %reduce-scatter.2.cloned.1.call-done), calls=%async_computation.3 | async-start | bytes 524288 | tf_op jit(solution)/shard_map/all_to_all | solution.py:250
Sparse Core Ops, SparseCore 0:
  9.5 43.5 all-gather.2
  63.3 31.9 all-reduce.1
  113.1 14.9 all-gather.4
  133.5 24.7 reduce-scatter.1
where the time goes:
time: 181 us
  waiting for transfers between devices  78.5 us (43%)
  blocking collectives  51.6 us (29%)
  between operations  14 us (8%)
  matrix products  13.2 us (7%)
  other arithmetic  10.8 us (6%)
  local copies, waits for them, and re-layouts  6.7 us (4%)
  starting transfers between devices  5.64 us (3%)
    psum x1, waiting for transfers between devices, body(): lax.psum(partial_value.astype(jnp.bfloat16), 'tp').astype(jnp.float32)  31.1 us
    all_gather x1, blocking collectives, body(): lax.all_gather(rot_key, 'sp', axis=0, tiled=True)  28.3 us
    reduce_scatter x1, waiting for transfers between devices, body(): lax.psum_scatter(partials.astype(jnp.bfloat16), 'tp', scatter_dimension=2...  24.9 us
    all_to_all x1, blocking collectives, body(): lax.all_to_all(placed.reshape(groups, capacity, column_rows.shape[1]), 's...  13.6 us
    all_to_all x1, blocking collectives, body(): lax.all_to_all(routed_weights, 'sp', split_axis=0, concat_axis=0, tiled=T...  9.66 us
    all_gather x1, waiting for transfers between devices, body(): lax.all_gather(latent_rows, 'sp', axis=0, tiled=True)  9.58 us
    all_to_all x1, waiting for transfers between devices, body(): lax.all_to_all(summed_rows, 'sp', split_axis=0, concat_axis=0, tiled=True)  8.74 us
    all_to_all x1, starting transfers between devices, body(): lax.all_to_all(summed_rows, 'sp', split_axis=0, concat_axis=0, tiled=True)  5.51 us
  transfers between devices with their start and end apart: 5, of which 5 were waited for; matrix products, arithmetic and copies ran while one was open for 4% of the time, Pallas kernels for 0%

commit v1 on v0

--- a/solution.py
+++ b/solution.py
@@ -194,7 +194,9 @@
     tp_size = lax.axis_size("tp")
     quarter = model_width // tp_size
     col_start = lax.axis_index("tp") * quarter
-    summed = lax.psum(partial_value.astype(jnp.bfloat16), "tp").astype(jnp.float32)
+    summed = jnp.sum(lax.all_gather(partial_value.astype(jnp.bfloat16), "tp"), axis=0).astype(
+        jnp.float32
+    )
     stream = (resid.astype(jnp.float32) + summed).astype(jnp.bfloat16)
     normed = rms_scale(stream, ffn_gain).astype(jnp.bfloat16)
     stream_cols = lax.dynamic_slice_in_dim(stream, col_start, quarter, 1)

time: 181 us -> 173 us (0.956)
  waiting for transfers between devices: 78.5 us -> 68.3 us
    psum x1 -> x0, waiting for transfers between devices: 31.1 us -> none  [body(): lax.psum(partial_value.astype(jnp.bfloat16), 'tp').astype(jnp.float32)]
    all_gather x0 -> x1, waiting for transfers between devices: none -> 20.2 us  [body(): lax.all_gather(partial_value.astype(jnp.bfloat16), 'tp')]
    reduce_sum x0 -> x1, other arithmetic: none -> 2.02 us  [body(): jnp.sum(lax.all_gather(partial_value.astype(jnp.bfloat16), 'tp'), axis=0)]
where the time goes in v1:
time: 173 us; the launch traced here: 172 us
  waiting for transfers between devices  68.3 us (39%)
  blocking collectives  53 us (31%)
  between operations  14.1 us (8%)
  matrix products  13.3 us (8%)
  other arithmetic  11.6 us (7%)
  local copies, waits for them, and re-layouts  6.09 us (4%)
  starting transfers between devices  5.63 us (3%)
    all_gather x1, blocking collectives, body(): lax.all_gather(rot_key, 'sp', axis=0, tiled=True)  28.3 us
    reduce_scatter x1, waiting for transfers between devices, body(): lax.psum_scatter(partials.astype(jnp.bfloat16), 'tp', scatter_dimension=2...  24.9 us
    all_gather x1, waiting for transfers between devices, body(): lax.all_gather(partial_value.astype(jnp.bfloat16), 'tp')  20.2 us
    all_to_all x1, blocking collectives, body(): lax.all_to_all(placed.reshape(groups, capacity, column_rows.shape[1]), 's...  14.7 us
    all_gather x1, waiting for transfers between devices, body(): lax.all_gather(latent_rows, 'sp', axis=0, tiled=True)  10.7 us
    all_to_all x1, blocking collectives, body(): lax.all_to_all(routed_weights, 'sp', split_axis=0, concat_axis=0, tiled=T...  9.92 us
    all_to_all x1, waiting for transfers between devices, body(): lax.all_to_all(summed_rows, 'sp', split_axis=0, concat_axis=0, tiled=True)  8.74 us
    all_to_all x1, starting transfers between devices, body(): lax.all_to_all(summed_rows, 'sp', split_axis=0, concat_axis=0, tiled=True)  5.51 us
  transfers between devices with their start and end apart: 5, of which 5 were waited for; matrix products, arithmetic and copies ran while one was open for 4% of the time, Pallas kernels for 0%

profile of v1, /device:TPU:0, one launch (start us, length us, event | category | flops | bytes accessed | tf_op | source)
XLA Modules:
  0.0 172.1 jit_solution(8464355583354757501)
XLA Ops:
  6.5 1.2 fusion.38
  7.7 1.7 fusion.40
  9.5 0.7 convert_element_type.132
  10.2 1.0 copy.74
  11.2 1.0 copy.75
  12.2 0.7 slice.38
  13.8 28.3 %all_gather.16 = bf16[1024,64]{0,1:T(8,128)(2,1)S(1)} all-gather(bf16[128,64]{0,1:T(8,128)(2,1)S(1)} %pad_maximum_fusion.2), channel_id=1, replica_groups=mesh['sp'=8,'tp'=4] {'sp'}, dimensions={0}, use_global_device_ids=true | all-gather | bytes 147456 | tf_op jit(solution)/shard_map/all_gather | solution.py:166
  42.2 10.7 %all-gather.5.cloned.1.call-done = bf16[1024,512]{1,0:T(8,128)(2,1)} async-done(((bf16[128,512]{1,0:T(8,128)(2,1)}), bf16[1024,512]{1,0:T(8,128)(2,1)}) %all-gather.5.cloned.1.call-update) | async-done | bytes 1048592 | tf_op jit(solution)/shard_map/all_gather | solution.py:165
  52.9 6.5 %conditional.1 = (f32[2,128]{1,0:T(2,128)S(1)}, f32[128,2,128]{0,2,1:T(8,128)S(1)}, f32[2,128]{1,0:T(2,128)S(1)}, f32[128,2,64]{0,2,1:T(8,128)S(1)}) conditional(s32[]{:T(128)} %bitcast.13, (s32[128]{0:T(128)S(1)}, s32[1024]{0:T(1024)S(1)}, bf16[1024,512]{1,0:T(8,128)(2,1)}, bf16[512,256]{1,0:T(8,128)(2,1)}, bf16[128,2,192]{0,2,1:T(8,128)(2,1)S(1)}, ...), branch_computations={%region_1.6_spmd, %region_6.7_spmd} | conditional | flops 1078953472 | bytes 26341008 | solution.py:182
  52.9 1.7 %convolution_convert_fusion.1 = bf16[1024,256]{0,1:T(8,128)(2,1)S(1)} fusion(bf16[1024,512]{1,0:T(8,128)(2,1)} %get-tuple-element.176, bf16[512,256]{1,0:T(8,128)(2,1)} %get-tuple-element.203), kind=kOutput, calls=%fused_computation.14 | convolution fusion | flops 268697600 | bytes 1835008 | tf_op jit(solution)/shard_map/while/body/eval_jaxpr/cond/branch_0_fun/dot_general | solution.py:91
  56.0 0.5 convolution_convert_fusion.3
  58.6 0.5 convolution_convert_fusion
  59.5 1.6 fusion.54
  61.1 1.1 fusion.23
  62.6 0.8 dynamic-slice
  63.5 20.2 %all-gather.9.cloned.1.call-done = bf16[512,2048]{1,0:T(8,128)(2,1)} async-done(((bf16[128,2048]{1,0:T(8,128)(2,1)}), bf16[512,2048]{1,0:T(8,128)(2,1)}) %all-gather.9.cloned.1.call-update) | async-done | bytes 2097168 | tf_op jit(solution)/shard_map/all_gather | solution.py:197
  83.7 2.0 %reduce_sum.80 = bf16[128,2048]{1,0:T(8,128)(2,1)S(1)} reduce(bf16[4,128,2048]{2,1,0:T(8,128)(2,1)} %bitcast.107, bf16[]{:T(256)} %constant.81.clone.1), dimensions={0}, to_apply=%region_7.0 | reduce | flops 786432 | bytes 2621442 | tf_op jit(solution)/shard_map/reduce_sum | solution.py:197
  85.7 1.3 multiply_reduce_fusion
  87.1 1.1 convert_element_type.144
  88.2 1.6 scatter_custom_fusion
  89.8 14.7 %all_to_all.15 = bf16[8,32,512]{2,1,0:T(8,128)(2,1)} all-to-all(bf16[8,32,512]{2,1,0:T(8,128)(2,1)S(1)} %bitcast.109), channel_id=1, replica_groups=mesh['sp'=8,'tp'=4] {'sp'}, dimensions={0} | all-to-all | bytes 524288 | tf_op jit(solution)/shard_map/all_to_all | solution.py:224
  104.8 0.9 scatter_custom_fusion.1
  105.8 9.9 %all_to_all.16 = bf16[8,32,4]{1,2,0:T(4,128)(2,1)S(1)} all-to-all(bf16[8,32,4]{1,2,0:T(4,128)(2,1)S(1)} %copy.78), channel_id=1, replica_groups=mesh['sp'=8,'tp'=4] {'sp'}, dimensions={0} | all-to-all | bytes 4096 | tf_op jit(solution)/shard_map/all_to_all | solution.py:242
  115.8 3.6 %all-gather.7.cloned.1.call-done = bf16[8,32,2048]{2,1,0:T(8,128)(2,1)} async-done(((bf16[8,32,512]{2,1,0:T(8,128)(2,1)}), bf16[8,32,2048]{2,1,0:T(8,128)(2,1)}) %all-gather.7.cloned.1.call-update) | async-done | bytes 1048592 | tf_op jit(solution)/shard_map/all_gather | solution.py:223
  119.5 2.8 %fusion.27 = f32[256,4,128]{2,0,1:T(8,128)S(1)} fusion(bf16[256,2048,1]{1,0,2:T(8,128)(2,1)} %bitcast.121, bf16[1,4,2048,128]{3,2,1,0:T(8,128)(2,1)} %param.39), kind=kOutput, calls=%fused_computation.49 | convolution fusion | flops 536870912 | bytes 3670016 | tf_op jit(solution)/shard_map/rd,edf->ref/dot_general | solution.py:237
  122.3 0.7 fusion.35
  123.0 1.7 %fusion.22 = bf16[8,32,2048]{2,1,0:T(8,128)(2,1)} fusion(bf16[8,32,4,128]{3,1,0,2:T(8,128)(2,1)S(1)} %bitcast.123, bf16[1,4,128,2048]{3,2,1,0:T(8,128)(2,1)S(1)} %copy-done), kind=kOutput, calls=%fused_computation.43 | convolution fusion | flops 537395200 | bytes 3407872 | tf_op jit(solution)/shard_map/ref,efd->rd/dot_general | solution.py:247
  124.8 24.9 %reduce-scatter.2.cloned.1.call-done = bf16[8,32,512]{2,1,0:T(8,128)(2,1)} async-done(((bf16[8,32,2048]{2,1,0:T(8,128)(2,1)}), bf16[8,32,512]{2,1,0:T(8,128)(2,1)}) %reduce-scatter.2.cloned.1.call-update) | async-done | bytes 262160 | tf_op jit(solution)/shard_map/reduce_scatter | solution.py:249
  149.7 5.5 %all-to-all-start.2 = ((bf16[8,32,512]{2,1,0:T(8,128)(2,1)}), bf16[8,32,512]{2,1,0:T(8,128)(2,1)S(1)}, u32[]{:S(2)}, u32[]{:S(2)}) async-start(bf16[8,32,512]{2,1,0:T(8,128)(2,1)} %reduce-scatter.2.cloned.1.call-done), calls=%async_computation.3 | async-start | bytes 524288 | tf_op jit(solution)/shard_map/all_to_all | solution.py:252
  155.2 8.7 %all-to-all-done.2 = bf16[8,32,512]{2,1,0:T(8,128)(2,1)S(1)} async-done(((bf16[8,32,512]{2,1,0:T(8,128)(2,1)}), bf16[8,32,512]{2,1,0:T(8,128)(2,1)S(1)}, u32[]{:S(2)}, u32[]{:S(2)}) %all-to-all-start.2) | async-done | bytes 262176 | tf_op jit(solution)/shard_map/all_to_all | solution.py:252
  164.0 0.8 gather_fusion
  164.8 0.7 add_convert_fusion.1
  (74 shorter events, 5.0 us)
Async XLA Ops:
  6.5 116.5 %copy-start = (bf16[1,4,128,2048]{3,2,1,0:T(8,128)(2,1)S(1)}, bf16[1,4,128,2048]{3,2,1,0:T(8,128)(2,1)}, u32[]{:S(2)}) copy-start(bf16[1,4,128,2048]{3,2,1,0:T(8,128)(2,1)} %param.41) | copy-start | bytes 6291460
  6.5 46.4 %all-gather.5.cloned.1.call-start = ((), (), s32[]{:S(2)}) async-start(), calls=%async_computation.4 | async-start | bytes 1179648 | tf_op jit(solution)/shard_map/all_gather | solution.py:165
  9.4 74.3 %all-gather.9.cloned.1.call-start = ((), (), s32[]{:S(2)}) async-start(), calls=%async_computation.7 | async-start | bytes 2621440 | tf_op jit(solution)/shard_map/all_gather | solution.py:197
  54.8 1.2 copy-start.1
  54.8 1.2 copy-start.4
  56.8 0.9 copy-start.5
  57.2 1.3 copy-start.3
  59.4 1.7 copy-start.2
  59.5 2.8 %copy-start.7 = (s32[128]{0:T(128)S(1)}, s32[128]{0:T(128)}, u32[]{:S(2)}) copy-start(s32[128]{0:T(128)} %param.35) | copy-start | bytes 1540
  62.2 57.2 %all-gather.7.cloned.1.call-start = ((), (), s32[]{:S(2)}) async-start(), calls=%async_computation.5 | async-start | bytes 1310720 | tf_op jit(solution)/shard_map/all_gather | solution.py:223
  85.7 18.9 %copy-start.6 = (f32[128,2]{0,1:T(2,128)S(1)}, f32[128,2]{0,1:T(2,128)}, u32[]{:S(2)}) copy-start(f32[128,2]{0,1:T(2,128)} %param.38) | copy-start | bytes 3076
  85.7 18.9 %copy-start.9 = (f32[128]{0:T(128)S(1)}, f32[128]{0:T(128)}, u32[]{:S(2)}) copy-start(f32[128]{0:T(128)} %param.37) | copy-start | bytes 1540
  85.7 18.9 %copy-start.8 = (s32[128,2]{0,1:T(2,128)S(1)}, s32[128,2]{0,1:T(2,128)}, u32[]{:S(2)}) copy-start(s32[128,2]{0,1:T(2,128)} %param.36) | copy-start | bytes 3076
  104.5 45.2 %reduce-scatter.2.cloned.1.call-start = ((), (), s32[]{:S(2)}) async-start(), calls=%async_computation.6 | async-start | bytes 1310720 | tf_op jit(solution)/shard_map/reduce_scatter | solution.py:249
  119.5 2.8 %copy-start.10 = (bf16[1,4,2048,128]{3,2,1,0:T(8,128)(2,1)S(1)}, bf16[1,4,2048,128]{3,2,1,0:T(8,128)(2,1)}, u32[]{:S(2)}) copy-start(bf16[1,4,2048,128]{3,2,1,0:T(8,128)(2,1)} %param.40) | copy-start | bytes 6291460
  119.5 2.8 %copy-start.11 = (bf16[8,32,2048]{2,1,0:T(8,128)(2,1)S(1)}, bf16[8,32,2048]{2,1,0:T(8,128)(2,1)}, u32[]{:S(2)}) copy-start(bf16[8,32,2048]{2,1,0:T(8,128)(2,1)} %all-gather.7.cloned.1.call-done) | copy-start | bytes 3145732
  149.7 14.3 %all-to-all-start.2 = ((bf16[8,32,512]{2,1,0:T(8,128)(2,1)}), bf16[8,32,512]{2,1,0:T(8,128)(2,1)S(1)}, u32[]{:S(2)}, u32[]{:S(2)}) async-start(bf16[8,32,512]{2,1,0:T(8,128)(2,1)} %reduce-scatter.2.cloned.1.call-done), calls=%async_computation.3 | async-start | bytes 524288 | tf_op jit(solution)/shard_map/all_to_all | solution.py:252
Sparse Core Ops, SparseCore 0:
  9.5 43.3 all-gather.4
  62.4 21.2 all-gather.8
  104.7 14.7 all-gather.6
  124.9 24.7 reduce-scatter.1
